TPU v7x, 32 devices: a whole 2x2x4 slice. The times are simulated.
32 devices in a mesh: sp: 8 (over z, core), tp: 4 (over y, x).
Axes of the slice: x: 2, y: 2, z: 4, core: 2. Of those that a mesh axis runs over, the one named last changes fastest.
Arguments:
- tokens: bfloat16 [2048, 4096], P('sp'), may hold values from -6 to 6
- norm_gain: float32 [2, 4096], replicated, may hold values from 0.1 to 1.9
- w_outer: bfloat16 [2, 4096, 1024], P(None, 'sp', 'tp'), may hold values from -0.09375 to 0.09375
- w_inner: bfloat16 [2, 4096, 1024], P(None, 'sp', 'tp'), may hold values from -0.09375 to 0.09375
- w_value: bfloat16 [2, 4096, 1024], P(None, 'sp', 'tp'), may hold values from -0.09375 to 0.09375
- w_back: bfloat16 [2, 1024, 4096], P(None, 'sp', 'tp'), may hold values from -0.1875 to 0.1875
- taps: float32 [2, 3, 1024], P(None, None, 'tp'), may hold values from -3 to 3
Outputs:
- result: bfloat16 [2048, 4096], P('sp', 'tp')
All inputs are finite; a program needn't handle non-finite values.
Results may differ from a plain program's by a relative error of at most 0.022.
Values may be sent and summed in bfloat16 or wider, within the bound.
A program may use at most 64 MiB of HBM per device.

v0:
```python
import jax
import jax.numpy as jnp
from jax import lax
from jax.sharding import PartitionSpec as P

eps = 1e-06


def shifted(block, axis, distance):
    devices = range(lax.axis_size(axis))
    route = [(i - distance, i) for i in devices if i - distance in devices]
    return lax.ppermute(block, axis, route)


def per_device(tokens, norm_gain, w_outer, w_inner, w_value, w_back, taps):
    layers = w_outer.shape[0]
    count = tokens.shape[0]
    feats = w_back.shape[2]
    own = lax.axis_index("tp")
    held = (
        lax.all_gather(w_outer, "sp", axis=1, tiled=True),
        lax.all_gather(w_inner, "sp", axis=1, tiled=True),
        lax.all_gather(w_value, "sp", axis=1, tiled=True),
        lax.all_gather(w_back, "sp", axis=1, tiled=True),
    )
    current = tokens
    resid = lax.dynamic_slice_in_dim(tokens, own * feats, feats, 1)
    for layer in range(layers):
        if layer > 0:
            current = lax.all_gather(resid, "tp", axis=1, tiled=True)
        xf = current.astype(jnp.float32)
        normed = (
            xf * lax.rsqrt(jnp.mean(xf * xf, axis=-1, keepdims=True) + eps) * norm_gain[layer]
        ).astype(jnp.bfloat16)
        outer = jnp.dot(normed, held[0][layer], preferred_element_type=jnp.float32)
        inner = jnp.dot(normed, held[1][layer], preferred_element_type=jnp.float32)
        value = jnp.dot(normed, held[2][layer], preferred_element_type=jnp.float32)
        outer = outer.astype(jnp.bfloat16)
        inner = inner.astype(jnp.bfloat16)
        value = value.astype(jnp.bfloat16)
        mixed = (inner.astype(jnp.float32) * value.astype(jnp.float32)).astype(jnp.bfloat16)
        before = shifted(mixed[count - 2 :], "sp", 1)
        padded = jnp.concatenate([before, mixed], axis=0).astype(jnp.float32)
        conv = (
            taps[layer, 0] * padded[:count]
            + taps[layer, 1] * padded[1 : count + 1]
            + taps[layer, 2] * padded[2:]
        )
        gated = (outer.astype(jnp.float32) * conv).astype(jnp.bfloat16)
        whole = lax.all_gather(gated, "tp", axis=1, tiled=True)
        proj = jnp.dot(whole, held[3][layer], preferred_element_type=jnp.float32)
        resid = (resid.astype(jnp.float32) + proj).astype(jnp.bfloat16)
    return resid


def solution(mesh):
    in_specs = (
        P("sp", None),
        P(),
        P(None, "sp", "tp"),
        P(None, "sp", "tp"),
        P(None, "sp", "tp"),
        P(None, "sp", "tp"),
        P(None, None, "tp"),
    )
    out_specs = P("sp", "tp")
    return jax.shard_map(
        per_device, mesh=mesh, in_specs=in_specs, out_specs=out_specs, check_vma=False
    )
```

profile of v0, /device:TPU:0, one launch (start us, length us, event | category | flops | bytes accessed | tf_op | source)
XLA Modules:
  0.0 271.6 jit_solution(8346042315905669766)
XLA Ops:
  6.5 0.7 all-gather.10.cloned.1.call-update
  7.3 0.7 all-gather.8.cloned.1.call-update
  9.4 2.1 fusion
  11.5 47.1 %all-gather.10.cloned.1.call-done = bf16[2,4096,256]{2,1,0:T(8,128)(2,1)} async-done(((bf16[2,512,256]{2,1,0:T(8,128)(2,1)}), bf16[2,4096,256]{2,1,0:T(8,128)(2,1)}) %all-gather.10.cloned.1.call-update) | async-done | bytes 4194320 | tf_op jit(solution)/shard_map/all_gather | solution.py:23
  58.6 2.4 fusion.27
  60.9 44.9 %all-gather.8.cloned.1.call-done = bf16[2,4096,256]{2,1,0:T(8,128)(2,1)} async-done(((bf16[2,512,256]{2,1,0:T(8,128)(2,1)}), bf16[2,4096,256]{2,1,0:T(8,128)(2,1)}) %all-gather.8.cloned.1.call-update) | async-done | bytes 4194320 | tf_op jit(solution)/shard_map/all_gather | solution.py:22
  105.9 2.4 fusion.25
  108.3 2.1 collective-permute-start
  110.4 0.8 collective-permute-done
  111.2 42.0 %all-gather.6.cloned.1.call-done = bf16[2,4096,256]{2,1,0:T(8,128)(2,1)} async-done(((bf16[2,512,256]{2,1,0:T(8,128)(2,1)}), bf16[2,4096,256]{2,1,0:T(8,128)(2,1)}) %all-gather.6.cloned.1.call-update) | async-done | bytes 4194320 | tf_op jit(solution)/shard_map/all_gather | solution.py:21
  153.2 2.4 fusion.21
  155.6 14.2 %all_gather.24 = bf16[256,1024]{1,0:T(8,128)(2,1)S(1)} all-gather(bf16[256,256]{1,0:T(8,128)(2,1)S(1)} %fusion.21), channel_id=1, replica_groups=mesh['sp'=8,'tp'=4] {'tp'}, dimensions={1}, use_global_device_ids=true | all-gather | bytes 655360 | tf_op jit(solution)/shard_map/all_gather | solution.py:50
  169.8 30.6 %all-gather.12.cloned.1.call-done = bf16[2,1024,1024]{2,1,0:T(8,128)(2,1)} async-done(((bf16[2,128,1024]{2,1,0:T(8,128)(2,1)}), bf16[2,1024,1024]{2,1,0:T(8,128)(2,1)}) %all-gather.12.cloned.1.call-update) | async-done | bytes 4194320 | tf_op jit(solution)/shard_map/all_gather | solution.py:24
  200.4 3.1 %fusion.17 = bf16[256,1024]{1,0:T(8,128)(2,1)} fusion(bf16[256,1024]{1,0:T(8,128)(2,1)S(1)} %all_gather.24, bf16[2,1024,1024]{2,1,0:T(8,128)(2,1)} %all-gather.12.cloned.1.call-done, bf16[256,4096]{1,0:T(8,128)(2,1)S(1)} %copy-done, s32[]{:T(128)S(6)} %select_n.3), kind=kOutput, calls=%fused_computation.29 | convolution fusion | flops 537657344 | bytes 3670020 | tf_op jit(solution)/shard_map/dot_general | solution.py:51
  203.5 34.1 %all-gather.14.cloned.1.call-done = bf16[256,4096]{1,0:T(8,128)(2,1)} async-done(((bf16[256,1024]{1,0:T(8,128)(2,1)}), bf16[256,4096]{1,0:T(8,128)(2,1)}) %all-gather.14.cloned.1.call-update) | async-done | bytes 2097168 | tf_op jit(solution)/shard_map/all_gather | solution.py:30
  237.6 2.1 fusion.3
  239.7 3.1 %fusion.37 = f32[256,256]{1,0:T(8,128)S(1)} fusion(bf16[2,4096,256]{2,1,0:T(8,128)(2,1)} %all-gather.10.cloned.1.call-done, bf16[256,4096]{1,0:T(8,128)(2,1)} %all-gather.14.cloned.1.call-done, f32[4096]{0:T(1024)S(1)} %bitcast.82, f32[256]{0:T(256)S(1)} %add_rsqrt_fusion), kind=kOutput, calls=%fused_computation.49 | convolution fusion | flops 541196288 | bytes 4473856 | tf_op jit(solution)/shard_map/dot_general | solution.py:37
  242.9 0.9 copy-done.7
  243.8 0.8 fusion.35
  244.6 1.7 collective-permute-start.1
  246.3 0.8 collective-permute-done.1
  247.2 0.8 fusion.31
  248.0 15.6 %all_gather.27 = bf16[256,1024]{1,0:T(8,128)(2,1)S(1)} all-gather(bf16[256,256]{1,0:T(8,128)(2,1)S(1)} %fusion.31), channel_id=1, replica_groups=mesh['sp'=8,'tp'=4] {'tp'}, dimensions={1}, use_global_device_ids=true | all-gather | bytes 655360 | tf_op jit(solution)/shard_map/all_gather | solution.py:50
  263.6 1.5 fusion.16
  (31 shorter events, 1.5 us)
Async XLA Ops:
  6.5 52.0 %copy-start = (bf16[256,4096]{1,0:T(8,128)(2,1)S(1)}, bf16[256,4096]{1,0:T(8,128)(2,1)}, u32[]{:S(2)}) copy-start(bf16[256,4096]{1,0:T(8,128)(2,1)} %param.7) | copy-start | bytes 6291460
  6.5 4.9 %copy-start.3 = (f32[2,4096]{1,0:T(2,128)S(1)}, f32[2,4096]{1,0:T(2,128)}, u32[]{:S(2)}) copy-start(f32[2,4096]{1,0:T(2,128)} %param.8) | copy-start | bytes 98308
  6.5 52.0 %all-gather.10.cloned.1.call-start = ((), (), s32[]{:S(2)}) async-start(), calls=%async_computation.2 | async-start | bytes 4718592 | tf_op jit(solution)/shard_map/all_gather | solution.py:23
  7.3 98.6 %all-gather.8.cloned.1.call-start = ((), (), s32[]{:S(2)}) async-start(), calls=%async_computation.1 | async-start | bytes 4718592 | tf_op jit(solution)/shard_map/all_gather | solution.py:22
  8.0 145.2 %all-gather.6.cloned.1.call-start = ((), (), s32[]{:S(2)}) async-start(), calls=%async_computation | async-start | bytes 4718592 | tf_op jit(solution)/shard_map/all_gather | solution.py:21
  8.7 191.6 %all-gather.12.cloned.1.call-start = ((), (), s32[]{:S(2)}) async-start(), calls=%async_computation.3 | async-start | bytes 4718592 | tf_op jit(solution)/shard_map/all_gather | solution.py:24
  9.3 228.3 %all-gather.14.cloned.1.call-start = ((), (), s32[]{:S(2)}) async-start(), calls=%async_computation.4 | async-start | bytes 2621440 | tf_op jit(solution)/shard_map/all_gather | solution.py:30
  60.9 49.5 %copy-start.4 = (f32[2,3,256]{2,0,1:T(2,128)S(1)}, f32[2,3,256]{2,0,1:T(2,128)}, u32[]{:S(2)}) copy-start(f32[2,3,256]{2,0,1:T(2,128)} %param.13) | copy-start | bytes 18436
  108.3 2.9 %collective-permute-start = (bf16[2,256]{1,0:T(2,128)(2,1)S(1)}, bf16[2,256]{1,0:T(2,128)(2,1)S(1)}, u32[]{:S(2)}, u32[]{:S(2)}) collective-permute-start(bf16[2,256]{1,0:T(2,128)(2,1)S(1)} %slice.99), channel_id=1, source_target_pairs={{0,4},{4,8},{8,12},{12,16},{16,20},{20,24},{24,28},{1,5},{5,9},{9,... | collective-permute-start | bytes 3080 | tf_op jit(solution)/shard_map/ppermute | solution.py:12
  239.7 3.2 %copy-start.1 = (bf16[256,4096]{1,0:T(8,128)(2,1)S(1)}, bf16[256,4096]{1,0:T(8,128)(2,1)}, u32[]{:S(2)}) copy-start(bf16[256,4096]{1,0:T(8,128)(2,1)} %all-gather.14.cloned.1.call-done) | copy-start | bytes 6291460
  239.7 4.1 %copy-start.7 = (bf16[2,4096,256]{2,1,0:T(8,128)(2,1)S(1)}, bf16[2,4096,256]{2,1,0:T(8,128)(2,1)}, u32[]{:S(2)}) copy-start(bf16[2,4096,256]{2,1,0:T(8,128)(2,1)} %all-gather.8.cloned.1.call-done) | copy-start | bytes 12582916
  243.8 3.4 %copy-start.6 = (bf16[2,4096,256]{2,1,0:T(8,128)(2,1)S(1)}, bf16[2,4096,256]{2,1,0:T(8,128)(2,1)}, u32[]{:S(2)}) copy-start(bf16[2,4096,256]{2,1,0:T(8,128)(2,1)} %all-gather.6.cloned.1.call-done) | copy-start | bytes 12582916
  244.6 2.5 collective-permute-start.1
  247.2 16.4 %copy-start.2 = (bf16[256,1024]{1,0:T(8,128)(2,1)S(1)}, bf16[256,1024]{1,0:T(8,128)(2,1)}, u32[]{:S(2)}) copy-start(bf16[256,1024]{1,0:T(8,128)(2,1)} %fusion.17) | copy-start | bytes 1572868
  247.2 16.4 %copy-start.5 = (bf16[2,1024,1024]{2,1,0:T(8,128)(2,1)S(1)}, bf16[2,1024,1024]{2,1,0:T(8,128)(2,1)}, u32[]{:S(2)}) copy-start(bf16[2,1024,1024]{2,1,0:T(8,128)(2,1)} %all-gather.12.cloned.1.call-done) | copy-start | bytes 12582916
Sparse Core Ops, SparseCore 0:
  8.9 49.5 all-gather.9
  60.2 45.6 all-gather.7
  107.5 45.6 all-gather.5
  154.7 45.6 all-gather.11
  203.6 33.9 all-gather.13
where the time goes:
time: 272 us
  waiting for transfers between devices  203 us (75%)
  blocking collectives  29.8 us (11%)
  matrix products  16.4 us (6%)
  between operations  13.3 us (5%)
  other arithmetic  4.24 us (2%)
  starting transfers between devices  4 us (1%)
    all_gather x1, waiting for transfers between devices, per_device(): lax.all_gather(w_value, 'sp', axis=1, tiled=True)  47.1 us
    all_gather x1, waiting for transfers between devices, per_device(): lax.all_gather(w_inner, 'sp', axis=1, tiled=True)  44.9 us
    all_gather x1, waiting for transfers between devices, per_device(): lax.all_gather(w_outer, 'sp', axis=1, tiled=True)  42 us
    all_gather x1, waiting for transfers between devices, per_device(): current = lax.all_gather(resid, 'tp', axis=1, tiled=True)  34.1 us
    all_gather x1, waiting for transfers between devices, per_device(): lax.all_gather(w_back, 'sp', axis=1, tiled=True)  30.6 us
    all_gather x2, blocking collectives, per_device(): whole = lax.all_gather(gated, 'tp', axis=1, tiled=True)  29.8 us
    dot_general x2, matrix products, per_device(): value = jnp.dot(normed, held[2][layer], preferred_element_type=jnp.float32)  5.48 us
  transfers between devices with their start and end apart: 7, of which 7 were waited for; matrix products, arithmetic and copies ran while one was open for 3% of the time, Pallas kernels for 0%

commit v1 on v0

--- a/solution.py
+++ b/solution.py
@@ -19,7 +19,7 @@
     own = lax.axis_index("tp")
     held = (
         lax.all_gather(w_outer, "sp", axis=1, tiled=True),
-        lax.all_gather(w_inner, "sp", axis=1, tiled=True),
+        jnp.concatenate(lax.all_gather(w_inner, "sp"), axis=1),
         lax.all_gather(w_value, "sp", axis=1, tiled=True),
         lax.all_gather(w_back, "sp", axis=1, tiled=True),
     )

time: 272 us -> 271 us (level)
  local copies, waits for them, and re-layouts: 0.99 us -> 4.15 us
  waiting for transfers between devices: 203 us -> 200 us
    all_gather x1, waiting for transfers between devices: 47.1 us -> 42.4 us  [per_device(): lax.all_gather(w_value, 'sp', axis=1, tiled=True)]
    slice x0 -> x1, local copies, waits for them, and re-layouts: none -> 4.07 us  [per_device(): inner = jnp.dot(normed, held[1][layer], preferred_element_type=jnp.float32)]
  transfers between devices with their start and end apart: 7 -> 7, of which waited for: 7 -> 7; matrix products, arithmetic and copies ran while one was open for 3% -> 4% of each run, Pallas kernels for 0% -> 0%
where the time goes in v1:
time: 271 us
  waiting for transfers between devices  200 us (74%)
  blocking collectives  29.8 us (11%)
  matrix products  15 us (6%)
  between operations  13.3 us (5%)
  other arithmetic  4.4 us (2%)
  local copies, waits for them, and re-layouts  4.15 us (2%)
  starting transfers between devices  3.98 us (1%)
    all_gather x1, waiting for transfers between devices, per_device(): lax.all_gather(w_inner, 'sp')  47.1 us
    all_gather x1, waiting for transfers between devices, per_device(): lax.all_gather(w_value, 'sp', axis=1, tiled=True)  42.4 us
    all_gather x1, waiting for transfers between devices, per_device(): lax.all_gather(w_outer, 'sp', axis=1, tiled=True)  41.9 us
    all_gather x1, waiting for transfers between devices, per_device(): current = lax.all_gather(resid, 'tp', axis=1, tiled=True)  34.1 us
    all_gather x1, waiting for transfers between devices, per_device(): lax.all_gather(w_back, 'sp', axis=1, tiled=True)  30.5 us
    all_gather x2, blocking collectives, per_device(): whole = lax.all_gather(gated, 'tp', axis=1, tiled=True)  29.8 us
  transfers between devices with their start and end apart: 7, of which 7 were waited for; matrix products, arithmetic and copies ran while one was open for 4% of the time, Pallas kernels for 0%

profile of v1, /device:TPU:0, one launch (start us, length us, event | category | flops | bytes accessed | tf_op | source)
XLA Modules:
  0.0 270.9 jit_solution(9452329579553354569)
XLA Ops:
  6.5 0.7 all-gather.15.cloned.1.call-update
  7.3 0.7 all-gather.9.cloned.1.call-update
  9.4 2.1 fusion
  11.5 47.1 %all-gather.15.cloned.1.call-done = bf16[16,512,256]{2,1,0:T(8,128)(2,1)} async-done(((bf16[2,512,256]{2,1,0:T(8,128)(2,1)}), bf16[16,512,256]{2,1,0:T(8,128)(2,1)}) %all-gather.15.cloned.1.call-update) | async-done | bytes 4194320 | tf_op jit(solution)/shard_map/all_gather | solution.py:22
  58.6 4.1 %fusion.44 = (bf16[1,8,512,256]{3,2,0,1:T(8,128)(2,1)S(1)}, bf16[1,8,512,256]{3,2,0,1:T(8,128)(2,1)}) fusion(bf16[2,8,512,256]{3,2,0,1:T(8,128)(2,1)} %bitcast.75), kind=kLoop, calls=%fused_computation.60 | loop fusion | bytes 8388608 | tf_op jit(solution)/shard_map/slice | solution.py:36
  62.6 0.8 fusion.33
  63.5 42.4 %all-gather.9.cloned.1.call-done = bf16[2,4096,256]{2,1,0:T(8,128)(2,1)} async-done(((bf16[2,512,256]{2,1,0:T(8,128)(2,1)}), bf16[2,4096,256]{2,1,0:T(8,128)(2,1)}) %all-gather.9.cloned.1.call-update) | async-done | bytes 4194320 | tf_op jit(solution)/shard_map/all_gather | solution.py:23
  105.9 2.4 fusion.23
  108.3 2.1 collective-permute-start
  110.4 0.8 collective-permute-done
  111.2 41.9 %all-gather.7.cloned.1.call-done = bf16[2,4096,256]{2,1,0:T(8,128)(2,1)} async-done(((bf16[2,512,256]{2,1,0:T(8,128)(2,1)}), bf16[2,4096,256]{2,1,0:T(8,128)(2,1)}) %all-gather.7.cloned.1.call-update) | async-done | bytes 4194320 | tf_op jit(solution)/shard_map/all_gather | solution.py:21
  153.2 2.4 fusion.19
  155.6 14.2 %all_gather.28 = bf16[256,1024]{1,0:T(8,128)(2,1)S(1)} all-gather(bf16[256,256]{1,0:T(8,128)(2,1)S(1)} %fusion.19), channel_id=1, replica_groups=mesh['sp'=8,'tp'=4] {'tp'}, dimensions={1}, use_global_device_ids=true | all-gather | bytes 655360 | tf_op jit(solution)/shard_map/all_gather | solution.py:50
  169.8 30.5 %all-gather.11.cloned.1.call-done = bf16[2,1024,1024]{2,1,0:T(8,128)(2,1)} async-done(((bf16[2,128,1024]{2,1,0:T(8,128)(2,1)}), bf16[2,1024,1024]{2,1,0:T(8,128)(2,1)}) %all-gather.11.cloned.1.call-update) | async-done | bytes 4194320 | tf_op jit(solution)/shard_map/all_gather | solution.py:24
  200.3 3.1 %fusion.15 = bf16[256,1024]{1,0:T(8,128)(2,1)} fusion(bf16[256,1024]{1,0:T(8,128)(2,1)S(1)} %all_gather.28, bf16[2,1024,1024]{2,1,0:T(8,128)(2,1)} %all-gather.11.cloned.1.call-done, bf16[256,4096]{1,0:T(8,128)(2,1)S(1)} %copy-done, s32[]{:T(128)S(6)} %select_n.3), kind=kOutput, calls=%fused_computation.25 | convolution fusion | flops 537657344 | bytes 3670020 | tf_op jit(solution)/shard_map/dot_general | solution.py:51
  203.5 34.1 %all-gather.13.cloned.1.call-done = bf16[256,4096]{1,0:T(8,128)(2,1)} async-done(((bf16[256,1024]{1,0:T(8,128)(2,1)}), bf16[256,4096]{1,0:T(8,128)(2,1)}) %all-gather.13.cloned.1.call-update) | async-done | bytes 2097168 | tf_op jit(solution)/shard_map/all_gather | solution.py:30
  237.6 2.2 fusion.3
  239.9 3.2 %fusion.32 = f32[256,256]{1,0:T(8,128)S(1)} fusion(bf16[4096,256]{1,0:T(8,128)(2,1)} %bitcast.76, bf16[256,4096]{1,0:T(8,128)(2,1)} %all-gather.13.cloned.1.call-done, f32[4096]{0:T(1024)S(1)} %bitcast.78, f32[256]{0:T(256)S(1)} %add_rsqrt_fusion), kind=kOutput, calls=%fused_computation.43 | convolution fusion | flops 541196288 | bytes 4473856 | tf_op jit(solution)/shard_map/dot_general | solution.py:36
  243.1 0.8 fusion.31
  243.9 1.7 collective-permute-start.1
  245.6 0.8 collective-permute-done.1
  246.5 0.8 fusion.27
  247.3 15.6 %all_gather.31 = bf16[256,1024]{1,0:T(8,128)(2,1)S(1)} all-gather(bf16[256,256]{1,0:T(8,128)(2,1)S(1)} %fusion.27), channel_id=1, replica_groups=mesh['sp'=8,'tp'=4] {'tp'}, dimensions={1}, use_global_device_ids=true | all-gather | bytes 655360 | tf_op jit(solution)/shard_map/all_gather | solution.py:50
  262.9 1.5 fusion.14
  (32 shorter events, 1.5 us)
Async XLA Ops:
  6.5 4.9 %copy-start.3 = (f32[2,4096]{1,0:T(2,128)S(1)}, f32[2,4096]{1,0:T(2,128)}, u32[]{:S(2)}) copy-start(f32[2,4096]{1,0:T(2,128)} %param.8) | copy-start | bytes 98308
  6.5 52.0 %all-gather.15.cloned.1.call-start = ((), (), s32[]{:S(2)}) async-start(), calls=%async_computation.4 | async-start | bytes 4718592 | tf_op jit(solution)/shard_map/all_gather | solution.py:22
  7.3 98.6 %all-gather.9.cloned.1.call-start = ((), (), s32[]{:S(2)}) async-start(), calls=%async_computation.1 | async-start | bytes 4718592 | tf_op jit(solution)/shard_map/all_gather | solution.py:23
  8.0 145.2 %all-gather.7.cloned.1.call-start = ((), (), s32[]{:S(2)}) async-start(), calls=%async_computation | async-start | bytes 4718592 | tf_op jit(solution)/shard_map/all_gather | solution.py:21
  8.7 191.6 %all-gather.11.cloned.1.call-start = ((), (), s32[]{:S(2)}) async-start(), calls=%async_computation.2 | async-start | bytes 4718592 | tf_op jit(solution)/shard_map/all_gather | solution.py:24
  9.3 228.3 %all-gather.13.cloned.1.call-start = ((), (), s32[]{:S(2)}) async-start(), calls=%async_computation.3 | async-start | bytes 2621440 | tf_op jit(solution)/shard_map/all_gather | solution.py:30
  58.6 4.1 %copy-start = (bf16[256,4096]{1,0:T(8,128)(2,1)S(1)}, bf16[256,4096]{1,0:T(8,128)(2,1)}, u32[]{:S(2)}) copy-start(bf16[256,4096]{1,0:T(8,128)(2,1)} %param.7) | copy-start | bytes 6291460
  63.4 47.0 %copy-start.4 = (f32[2,3,256]{2,0,1:T(2,128)S(1)}, f32[2,3,256]{2,0,1:T(2,128)}, u32[]{:S(2)}) copy-start(f32[2,3,256]{2,0,1:T(2,128)} %param.13) | copy-start | bytes 18436
  108.3 2.9 %collective-permute-start = (bf16[2,256]{1,0:T(2,128)(2,1)S(1)}, bf16[2,256]{1,0:T(2,128)(2,1)S(1)}, u32[]{:S(2)}, u32[]{:S(2)}) collective-permute-start(bf16[2,256]{1,0:T(2,128)(2,1)S(1)} %slice.101), channel_id=1, source_target_pairs={{0,4},{4,8},{8,12},{12,16},{16,20},{20,24},{24,28},{1,5},{5,9},{9,... | collective-permute-start | bytes 3080 | tf_op jit(solution)/shard_map/ppermute | solution.py:12
  237.6 5.5 %copy-start.1 = (bf16[256,4096]{1,0:T(8,128)(2,1)S(1)}, bf16[256,4096]{1,0:T(8,128)(2,1)}, u32[]{:S(2)}) copy-start(bf16[256,4096]{1,0:T(8,128)(2,1)} %all-gather.13.cloned.1.call-done) | copy-start | bytes 6291460
  237.6 5.5 %copy-start.7 = (bf16[2,4096,256]{2,1,0:T(8,128)(2,1)S(1)}, bf16[2,4096,256]{2,1,0:T(8,128)(2,1)}, u32[]{:S(2)}) copy-start(bf16[2,4096,256]{2,1,0:T(8,128)(2,1)} %all-gather.9.cloned.1.call-done) | copy-start | bytes 12582916
  243.1 3.4 %copy-start.6 = (bf16[2,4096,256]{2,1,0:T(8,128)(2,1)S(1)}, bf16[2,4096,256]{2,1,0:T(8,128)(2,1)}, u32[]{:S(2)}) copy-start(bf16[2,4096,256]{2,1,0:T(8,128)(2,1)} %all-gather.7.cloned.1.call-done) | copy-start | bytes 12582916
  243.9 2.5 collective-permute-start.1
  246.5 16.4 %copy-start.2 = (bf16[256,1024]{1,0:T(8,128)(2,1)S(1)}, bf16[256,1024]{1,0:T(8,128)(2,1)}, u32[]{:S(2)}) copy-start(bf16[256,1024]{1,0:T(8,128)(2,1)} %fusion.15) | copy-start | bytes 1572868
  246.5 16.4 %copy-start.5 = (bf16[2,1024,1024]{2,1,0:T(8,128)(2,1)S(1)}, bf16[2,1024,1024]{2,1,0:T(8,128)(2,1)}, u32[]{:S(2)}) copy-start(bf16[2,1024,1024]{2,1,0:T(8,128)(2,1)} %all-gather.11.cloned.1.call-done) | copy-start | bytes 12582916
Sparse Core Ops, SparseCore 0:
  8.9 49.5 all-gather.14
  60.2 45.6 all-gather.8
  107.5 45.6 all-gather.6
  154.6 45.6 all-gather.10
  203.6 33.9 all-gather.12
